TPU v7x, 32 devices: a whole 2x2x4 slice. The times are simulated.
32 devices in a mesh: ep: 8 (over z, x), tp: 4 (over y, core).
Axes of the slice: x: 2, y: 2, z: 4, core: 2. Of those that a mesh axis runs over, the one named last changes fastest.
Arguments:
- tokens: bfloat16 [1536, 2048], P('ep'), may hold values from -6 to 6
- cotangent: bfloat16 [1536, 2048], P('ep'), may hold values from -6 to 6
- routing: int32 [1536, 2], P('ep'), may hold values from 0 to 7, all different within a row; in each aligned block of 192 rows (0 to 191, 192 to 383, ...) at most 60 rows name the same one
- route_weights: float32 [1536, 2], P('ep'), may hold values from 0.1 to 1
- w_gate: bfloat16 [8, 2048, 2048], P('ep', None, 'tp'), may hold values from -0.125 to 0.125
- w_up: bfloat16 [8, 2048, 2048], P('ep', None, 'tp'), may hold values from -0.125 to 0.125
- w_down: bfloat16 [8, 2048, 2048], P('ep', 'tp'), may hold values from -0.125 to 0.125
Outputs:
- grad_tokens: bfloat16 [1536, 2048], P('ep')
- grad_weights: bfloat16 [1536, 2], P('ep')
- grad_gate: bfloat16 [8, 2048, 2048], P('ep', None, 'tp')
- grad_up: bfloat16 [8, 2048, 2048], P('ep', None, 'tp')
- grad_down: bfloat16 [8, 2048, 2048], P('ep', 'tp')
Inputs may be any that keep to these rules, and one draw needn't show every extreme that they name: `routing`: each row names 2 different experts. Within the rows of one device no expert is named more than 60 times, and in every draw some expert is named exactly 60 times by some device's rows.
All inputs are finite; a program needn't handle non-finite values.
Results may differ from a plain program's by a relative error of at most 0.019.
Values may be sent and summed in bfloat16 or wider, within the bound.
No kernel may reach another device: no remote copies, remote signals or barrier semaphores. Data moves between devices by JAX's collectives and lax.ppermute only.
A program may use at most 64 MiB of HBM per device.

v0:
```python
import jax
import jax.numpy as jnp
from jax import lax
from jax.sharding import PartitionSpec as P


def slot_tables(routing, experts, capacity):
    flat = routing.reshape(-1)
    onehot = (flat[:, None] == jnp.arange(experts, dtype=jnp.int32)[None, :]).astype(jnp.int32)
    before = jnp.cumsum(onehot, axis=0) - onehot
    within = jnp.sum(before * onehot, axis=1)
    target = flat * capacity + within
    chosen = jnp.arange(experts * capacity, dtype=jnp.int32)[:, None] == target[None, :]
    return (target, chosen)


def on_device(tokens, cotangent, routing, route_weights, w_gate, w_up, w_down):
    experts = lax.axis_size("ep")
    local_tokens, top_count = routing.shape
    width = tokens.shape[1]
    capacity = max(2, (5 * local_tokens * top_count + 4 * experts - 1) // (4 * experts))
    slot_total = experts * capacity
    target, chosen = slot_tables(routing, experts, capacity)
    picked = chosen.reshape(slot_total, local_tokens, top_count).astype(jnp.float32)
    by_token = jnp.sum(picked, axis=2).astype(jnp.bfloat16)
    slot_weight = jnp.sum(picked * route_weights[None, :, :], axis=(1, 2)).astype(jnp.bfloat16)
    send_rows = jnp.dot(by_token, tokens, preferred_element_type=jnp.float32).astype(jnp.bfloat16)
    send_back = jnp.dot(by_token, cotangent, preferred_element_type=jnp.float32).astype(
        jnp.bfloat16
    )
    rows_in, weight_in = (
        lax.all_to_all(
            send_rows.reshape(experts, capacity, width),
            "ep",
            split_axis=0,
            concat_axis=0,
            tiled=True,
        ),
        lax.all_to_all(
            slot_weight.reshape(experts, capacity), "ep", split_axis=0, concat_axis=0, tiled=True
        ),
    )
    back_in = lax.all_to_all(
        send_back.reshape(experts, capacity, width), "ep", split_axis=0, concat_axis=0, tiled=True
    )
    rows = rows_in.reshape(slot_total, width)
    back = back_in.reshape(slot_total, width)
    weight = weight_in.reshape(slot_total, 1).astype(jnp.float32)
    wgate = w_gate[0]
    wup = w_up[0]
    wdown = w_down[0]
    pre_gate = jnp.dot(rows, wgate, preferred_element_type=jnp.float32)
    pre_up = jnp.dot(rows, wup, preferred_element_type=jnp.float32)
    along = jnp.einsum("rd,fd->rf", back, wdown, preferred_element_type=jnp.float32)
    gate_sig = jax.nn.sigmoid(pre_gate)
    gate_act = pre_gate * gate_sig
    hidden = gate_act * pre_up
    hidden_grad = weight * along
    gate_grad = (hidden_grad * pre_up * gate_sig * (1.0 + pre_gate * (1.0 - gate_sig))).astype(
        jnp.bfloat16
    )
    up_grad = (hidden_grad * gate_act).astype(jnp.bfloat16)
    scaled = (weight * hidden).astype(jnp.bfloat16)
    grad_gate = jnp.einsum("rd,rf->df", rows, gate_grad, preferred_element_type=jnp.float32).astype(
        jnp.bfloat16
    )
    grad_up = jnp.einsum("rd,rf->df", rows, up_grad, preferred_element_type=jnp.float32).astype(
        jnp.bfloat16
    )
    grad_down = jnp.einsum("rf,rd->fd", scaled, back, preferred_element_type=jnp.float32).astype(
        jnp.bfloat16
    )
    row_part = jnp.einsum(
        "rf,df->rd", gate_grad, wgate, preferred_element_type=jnp.float32
    ) + jnp.einsum("rf,df->rd", up_grad, wup, preferred_element_type=jnp.float32)
    slot_part = jnp.sum(hidden * along, axis=1)
    row_share = lax.psum_scatter(
        row_part.reshape(experts, capacity, width).astype(jnp.bfloat16),
        "tp",
        scatter_dimension=2,
        tiled=True,
    )
    slot_sum = lax.psum(slot_part.astype(jnp.bfloat16), "tp")
    back_grad = slot_sum.reshape(experts, capacity)
    home_rows, home_grad = (
        lax.all_to_all(row_share, "ep", split_axis=0, concat_axis=0, tiled=True),
        lax.all_to_all(back_grad, "ep", split_axis=0, concat_axis=0, tiled=True),
    )
    feature_part = jnp.einsum(
        "st,sd->td",
        by_token,
        home_rows.reshape(slot_total, home_rows.shape[2]),
        preferred_element_type=jnp.float32,
    ).astype(jnp.bfloat16)
    grad_tokens = lax.all_gather(feature_part, "tp", axis=1, tiled=True)
    grad_weights = home_grad.reshape(-1)[target].reshape(local_tokens, top_count)
    return (grad_tokens, grad_weights, grad_gate[None], grad_up[None], grad_down[None])


def solution(mesh):
    return jax.shard_map(
        on_device,
        mesh=mesh,
        in_specs=(
            P("ep", None),
            P("ep", None),
            P("ep", None),
            P("ep", None),
            P("ep", None, "tp"),
            P("ep", None, "tp"),
            P("ep", "tp", None),
        ),
        out_specs=(
            P("ep", None),
            P("ep", None),
            P("ep", None, "tp"),
            P("ep", None, "tp"),
            P("ep", "tp", None),
        ),
        check_vma=False,
    )
```

profile of v0, /device:TPU:0, one launch (start us, length us, event | category | flops | bytes accessed | tf_op | source)
XLA Modules:
  0.0 210.8 jit_solution(13199292134892144586)
XLA Ops:
  7.2 0.9 copy.26
  8.4 0.9 reduce-window.6
  9.9 0.9 select_reduce_fusion
  11.5 7.3 %all-to-all-start = ((bf16[8,1,60]{2,1,0:T(2,128)(2,1)}), bf16[8,1,60]{2,1,0:T(2,128)(2,1)S(1)}, u32[]{:S(2)}, u32[]{:S(2)}) async-start(bf16[8,1,60]{2,1,0:T(2,128)(2,1)} %convert_element_type.95), calls=%async_computation | async-start | bytes 8192 | tf_op jit(solution)/shard_map/all_to_all | solution.py:39
  18.8 3.1 %convolution_convert_fusion.3 = bf16[480,2048]{1,0:T(8,128)(2,1)} fusion(bf16[192,2048]{1,0:T(8,128)(2,1)} %param.7, bf16[480,192]{0,1:T(8,128)(2,1)S(1)} %get-tuple-element.21), kind=kOutput, calls=%fused_computation.5 | convolution fusion | flops 378470400 | bytes 2936832 | tf_op jit(solution)/shard_map/dot_general | solution.py:27
  21.9 2.7 %reshape.131 = bf16[8,60,2048]{2,1,0:T(8,128)(2,1)} reshape(bf16[480,2048]{1,0:T(8,128)(2,1)} %convolution_convert_fusion.3) | data formatting | bytes 3932160 | tf_op jit(solution)/shard_map/reshape | solution.py:33
  25.2 5.5 %all-to-all-start.2 = ((bf16[8,60,2048]{2,1,0:T(8,128)(2,1)}), bf16[8,60,2048]{2,1,0:T(8,128)(2,1)}, u32[]{:S(2)}, u32[]{:S(2)}) async-start(bf16[8,60,2048]{2,1,0:T(8,128)(2,1)} %reshape.131), calls=%async_computation.2 | async-start | bytes 4194304 | tf_op jit(solution)/shard_map/all_to_all | solution.py:32
  30.8 2.0 convolution_convert_fusion.4
  32.8 2.7 %reshape.129 = bf16[8,60,2048]{2,1,0:T(8,128)(2,1)} reshape(bf16[480,2048]{1,0:T(8,128)(2,1)} %convolution_convert_fusion.4) | data formatting | bytes 3932160 | tf_op jit(solution)/shard_map/reshape | solution.py:44
  35.5 43.1 %all-to-all-done.2 = bf16[8,60,2048]{2,1,0:T(8,128)(2,1)} async-done(((bf16[8,60,2048]{2,1,0:T(8,128)(2,1)}), bf16[8,60,2048]{2,1,0:T(8,128)(2,1)}, u32[]{:S(2)}, u32[]{:S(2)}) %all-to-all-start.2) | async-done | bytes 1966112 | tf_op jit(solution)/shard_map/all_to_all | solution.py:32
  78.5 4.3 %all-to-all-start.1 = ((bf16[8,60,2048]{2,1,0:T(8,128)(2,1)}), bf16[8,60,2048]{2,1,0:T(8,128)(2,1)}, u32[]{:S(2)}, u32[]{:S(2)}) async-start(bf16[8,60,2048]{2,1,0:T(8,128)(2,1)} %reshape.129), calls=%async_computation.1 | async-start | bytes 4194304 | tf_op jit(solution)/shard_map/all_to_all | solution.py:43
  83.0 2.7 %reshape.132 = bf16[480,2048]{1,0:T(8,128)(2,1)} reshape(bf16[8,60,2048]{2,1,0:T(8,128)(2,1)} %all-to-all-done.2) | data formatting | bytes 3932160 | tf_op jit(solution)/shard_map/reshape | solution.py:46
  85.8 3.8 %fusion.5 = f32[480,512]{1,0:T(8,128)} fusion(bf16[480,2048]{1,0:T(8,128)(2,1)} %reshape.132, bf16[1,2048,512]{2,1,0:T(8,128)(2,1)S(1)} %copy-done), kind=kOutput, calls=%fused_computation.12 | convolution fusion | flops 1006632960 | bytes 5046272 | tf_op jit(solution)/shard_map/dot_general | solution.py:52
  89.6 2.1 %fusion.8 = f32[480,512]{1,0:T(8,128)} fusion(bf16[480,2048]{1,0:T(8,128)(2,1)S(1)} %copy-done.3, bf16[1,2048,512]{2,1,0:T(8,128)(2,1)S(1)} %copy-done.1), kind=kOutput, calls=%fused_computation.15 | convolution fusion | flops 1006632960 | bytes 5046272 | tf_op jit(solution)/shard_map/dot_general | solution.py:53
  91.7 39.0 %all-to-all-done.1 = bf16[8,60,2048]{2,1,0:T(8,128)(2,1)} async-done(((bf16[8,60,2048]{2,1,0:T(8,128)(2,1)}), bf16[8,60,2048]{2,1,0:T(8,128)(2,1)}, u32[]{:S(2)}, u32[]{:S(2)}) %all-to-all-start.1) | async-done | bytes 1966112 | tf_op jit(solution)/shard_map/all_to_all | solution.py:43
  130.7 2.7 %reshape.130 = bf16[480,2048]{1,0:T(8,128)(2,1)} reshape(bf16[8,60,2048]{2,1,0:T(8,128)(2,1)} %all-to-all-done.1) | data formatting | bytes 3932160 | tf_op jit(solution)/shard_map/reshape | solution.py:47
  133.4 4.4 %multiply_reduce_fusion = (bf16[480]{0:T(512)(128)(2,1)S(1)}, bf16[480,512]{1,0:T(8,128)(2,1)S(1)}, bf16[480,512]{1,0:T(8,128)(2,1)S(1)}) fusion(f32[480,512]{1,0:T(8,128)} %fusion.8, f32[480,512]{1,0:T(8,128)} %fusion.5, f32[480]{0:T(512)S(1)} %reshape.136, bf16[480,2048]{1,0:T(8,128)(2,1)} %reshape.130, bf16[1,512,2048]{2,1,0:T(8,128)(2,1)} %param.13), kind=kOutput, calls=%fused_computation.21 | convolution fusion | flops 1010810368 | bytes 7015232 | tf_op jit(solution)/shard_map/rd,fd->rf/dot_general | solution.py:54
  137.8 1.2 fusion.3
  139.6 2.5 %add_convert_fusion = bf16[480,2048]{1,0:T(8,128)(2,1)} fusion(f32[480,2048]{1,0:T(8,128)S(1)} %fusion.3, bf16[480,512]{1,0:T(8,128)(2,1)S(1)} %get-tuple-element.24, bf16[1,2048,512]{2,1,0:T(8,128)(2,1)S(1)} %copy-done.2), kind=kOutput, calls=%fused_computation.1 | convolution fusion | flops 1008599040 | bytes 8486912 | tf_op jit(solution)/shard_map/rf,df->rd/dot_general | solution.py:75
  142.1 2.7 %convert_element_type.87 = bf16[8,60,2048]{2,1,0:T(8,128)(2,1)} reshape(bf16[480,2048]{1,0:T(8,128)(2,1)} %add_convert_fusion) | data formatting | bytes 3932160 | tf_op jit(solution)/shard_map/convert_element_type | solution.py:78
  145.1 5.7 %psum.7 = bf16[8,1,60]{2,0,1:T(8,128)(2,1)S(1)} all-reduce(bf16[8,1,60]{2,0,1:T(8,128)(2,1)S(1)} %all_to_all.23), channel_id=1, replica_groups=mesh['ep'=8,'tp'=4] {'tp'}, use_global_device_ids=true, to_apply=%region_7.8 | all-reduce | flops 480 | bytes 1920 | tf_op jit(solution)/shard_map/psum | solution.py:83
  151.4 4.9 %all-to-all-start.4 = ((bf16[8,1,60]{2,1,0:T(2,128)(2,1)}), bf16[8,1,60]{2,1,0:T(2,128)(2,1)S(1)}, u32[]{:S(2)}, u32[]{:S(2)}) async-start(bf16[8,1,60]{2,1,0:T(2,128)(2,1)} %copy.31), calls=%async_computation.5 | async-start | bytes 8192 | tf_op jit(solution)/shard_map/all_to_all | solution.py:87
  156.2 6.4 %all-to-all-done.4 = bf16[8,1,60]{2,1,0:T(2,128)(2,1)S(1)} async-done(((bf16[8,1,60]{2,1,0:T(2,128)(2,1)}), bf16[8,1,60]{2,1,0:T(2,128)(2,1)S(1)}, u32[]{:S(2)}, u32[]{:S(2)}) %all-to-all-start.4) | async-done | bytes 992 | tf_op jit(solution)/shard_map/all_to_all | solution.py:87
  162.6 12.6 %reduce-scatter.2.cloned.1.call-done = bf16[8,60,512]{2,1,0:T(8,128)(2,1)} async-done(((bf16[8,60,2048]{2,1,0:T(8,128)(2,1)}), bf16[8,60,512]{2,1,0:T(8,128)(2,1)}) %reduce-scatter.2.cloned.1.call-update) | async-done | bytes 491536 | tf_op jit(solution)/shard_map/reduce_scatter | solution.py:77
  175.2 5.5 %all-to-all-start.3 = ((bf16[8,60,512]{2,1,0:T(8,128)(2,1)}), bf16[8,60,512]{2,1,0:T(8,128)(2,1)S(1)}, u32[]{:S(2)}, u32[]{:S(2)}) async-start(bf16[8,60,512]{2,1,0:T(8,128)(2,1)} %reduce-scatter.2.cloned.1.call-done), calls=%async_computation.4 | async-start | bytes 1048576 | tf_op jit(solution)/shard_map/all_to_all | solution.py:86
  180.8 4.3 %fusion = bf16[1,2048,512]{2,1,0:T(8,128)(2,1)} fusion(bf16[480,2048]{1,0:T(8,128)(2,1)} %reshape.132, bf16[480,512]{1,0:T(8,128)(2,1)S(1)} %get-tuple-element.23), kind=kOutput, calls=%fused_computation.7 | convolution fusion | flops 1007681536 | bytes 4554752 | tf_op jit(solution)/shard_map/rd,rf->df/dot_general | solution.py:64
  185.1 2.6 %fusion.1 = bf16[1,2048,512]{2,1,0:T(8,128)(2,1)} fusion(bf16[480,2048]{1,0:T(8,128)(2,1)S(1)} %copy-done.4, bf16[480,512]{1,0:T(8,128)(2,1)S(1)} %copy-done.8), kind=kOutput, calls=%fused_computation.8 | convolution fusion | flops 1007681536 | bytes 4554752 | tf_op jit(solution)/shard_map/rd,rf->df/dot_general | solution.py:67
  187.8 2.8 %fusion.2 = bf16[1,512,2048]{2,1,0:T(8,128)(2,1)} fusion(bf16[480,2048]{1,0:T(8,128)(2,1)S(1)} %copy-done.5, f32[480]{0:T(512)S(1)} %reshape.136, f32[480,512]{1,0:T(8,128)S(1)} %copy-done.10, f32[480,512]{1,0:T(8,128)S(1)} %copy-done.9), kind=kOutput, calls=%fused_computation.9 | convolution fusion | flops 1009401856 | bytes 6031232 | tf_op jit(solution)/shard_map/rf,rd->fd/dot_general | solution.py:70
  190.7 2.8 %gather_fusion = bf16[384]{0:T(512)(128)(2,1)S(1)} fusion(bf16[480]{0:T(512)(128)(2,1)S(1)} %reshape.134, s32[1024]{0:T(1024)S(1)} %pad_clamp_fusion), kind=kCustom, calls=%fused_computation | custom fusion | bytes 3072 | tf_op jit(solution)/shard_map/gather | solution.py:96
  194.3 0.8 all-to-all-done.3
  195.4 7.7 %all_gather.3 = bf16[192,2048]{1,0:T(8,128)(2,1)S(1)} all-gather(bf16[192,512]{1,0:T(8,128)(2,1)S(1)} %convolution_convert_fusion.5), channel_id=1, replica_groups=mesh['ep'=8,'tp'=4] {'tp'}, dimensions={1}, use_global_device_ids=true | all-gather | bytes 983040 | tf_op jit(solution)/shard_map/all_gather | solution.py:95
  203.1 0.9 copy.34
  (48 shorter events, 5.0 us)
Async XLA Ops:
  7.2 78.6 %copy-start = (bf16[1,2048,512]{2,1,0:T(8,128)(2,1)S(1)}, bf16[1,2048,512]{2,1,0:T(8,128)(2,1)}, u32[]{:S(2)}) copy-start(bf16[1,2048,512]{2,1,0:T(8,128)(2,1)} %param.11) | copy-start | bytes 6291460
  11.5 13.7 %all-to-all-start = ((bf16[8,1,60]{2,1,0:T(2,128)(2,1)}), bf16[8,1,60]{2,1,0:T(2,128)(2,1)S(1)}, u32[]{:S(2)}, u32[]{:S(2)}) async-start(bf16[8,1,60]{2,1,0:T(2,128)(2,1)} %convert_element_type.95), calls=%async_computation | async-start | bytes 8192 | tf_op jit(solution)/shard_map/all_to_all | solution.py:39
  24.6 6.1 %copy-start.6 = (bf16[192,2048]{1,0:T(8,128)(2,1)S(1)}, bf16[192,2048]{1,0:T(8,128)(2,1)}, u32[]{:S(2)}) copy-start(bf16[192,2048]{1,0:T(8,128)(2,1)} %param.8) | copy-start | bytes 2359300
  25.2 53.3 %all-to-all-start.2 = ((bf16[8,60,2048]{2,1,0:T(8,128)(2,1)}), bf16[8,60,2048]{2,1,0:T(8,128)(2,1)}, u32[]{:S(2)}, u32[]{:S(2)}) async-start(bf16[8,60,2048]{2,1,0:T(8,128)(2,1)} %reshape.131), calls=%async_computation.2 | async-start | bytes 4194304 | tf_op jit(solution)/shard_map/all_to_all | solution.py:32
  78.5 52.2 %all-to-all-start.1 = ((bf16[8,60,2048]{2,1,0:T(8,128)(2,1)}), bf16[8,60,2048]{2,1,0:T(8,128)(2,1)}, u32[]{:S(2)}, u32[]{:S(2)}) async-start(bf16[8,60,2048]{2,1,0:T(8,128)(2,1)} %reshape.129), calls=%async_computation.1 | async-start | bytes 4194304 | tf_op jit(solution)/shard_map/all_to_all | solution.py:43
  82.9 92.3 %reduce-scatter.2.cloned.1.call-start = ((), (), s32[]{:S(2)}) async-start(), calls=%async_computation.6 | async-start | bytes 2621440 | tf_op jit(solution)/shard_map/reduce_scatter | solution.py:77
  85.8 3.8 %copy-start.1 = (bf16[1,2048,512]{2,1,0:T(8,128)(2,1)S(1)}, bf16[1,2048,512]{2,1,0:T(8,128)(2,1)}, u32[]{:S(2)}) copy-start(bf16[1,2048,512]{2,1,0:T(8,128)(2,1)} %param.12) | copy-start | bytes 6291460
  85.8 3.8 %copy-start.3 = (bf16[480,2048]{1,0:T(8,128)(2,1)S(1)}, bf16[480,2048]{1,0:T(8,128)(2,1)}, u32[]{:S(2)}) copy-start(bf16[480,2048]{1,0:T(8,128)(2,1)} %reshape.132) | copy-start | bytes 5898244
  137.8 1.3 copy-start.7
  137.8 1.8 copy-start.2
  151.4 11.3 %all-to-all-start.4 = ((bf16[8,1,60]{2,1,0:T(2,128)(2,1)}), bf16[8,1,60]{2,1,0:T(2,128)(2,1)S(1)}, u32[]{:S(2)}, u32[]{:S(2)}) async-start(bf16[8,1,60]{2,1,0:T(2,128)(2,1)} %copy.31), calls=%async_computation.5 | async-start | bytes 8192 | tf_op jit(solution)/shard_map/all_to_all | solution.py:87
  175.2 19.8 %all-to-all-start.3 = ((bf16[8,60,512]{2,1,0:T(8,128)(2,1)}), bf16[8,60,512]{2,1,0:T(8,128)(2,1)S(1)}, u32[]{:S(2)}, u32[]{:S(2)}) async-start(bf16[8,60,512]{2,1,0:T(8,128)(2,1)} %reduce-scatter.2.cloned.1.call-done), calls=%async_computation.4 | async-start | bytes 1048576 | tf_op jit(solution)/shard_map/all_to_all | solution.py:86
  180.7 4.4 %copy-start.4 = (bf16[480,2048]{1,0:T(8,128)(2,1)S(1)}, bf16[480,2048]{1,0:T(8,128)(2,1)}, u32[]{:S(2)}) copy-start(bf16[480,2048]{1,0:T(8,128)(2,1)} %reshape.132) | copy-start | bytes 5898244
  180.7 4.4 %copy-start.8 = (bf16[480,512]{1,0:T(8,128)(2,1)S(1)}, bf16[480,512]{1,0:T(8,128)(2,1)}, u32[]{:S(2)}) copy-start(bf16[480,512]{1,0:T(8,128)(2,1)} %copy-done.7) | copy-start | bytes 1474564
  185.1 2.7 %copy-start.5 = (bf16[480,2048]{1,0:T(8,128)(2,1)S(1)}, bf16[480,2048]{1,0:T(8,128)(2,1)}, u32[]{:S(2)}) copy-start(bf16[480,2048]{1,0:T(8,128)(2,1)} %reshape.130) | copy-start | bytes 5898244
  185.1 2.7 %copy-start.9 = (f32[480,512]{1,0:T(8,128)S(1)}, f32[480,512]{1,0:T(8,128)}, u32[]{:S(2)}) copy-start(f32[480,512]{1,0:T(8,128)} %fusion.5) | copy-start | bytes 2949124
  185.1 2.7 %copy-start.10 = (f32[480,512]{1,0:T(8,128)S(1)}, f32[480,512]{1,0:T(8,128)}, u32[]{:S(2)}) copy-start(f32[480,512]{1,0:T(8,128)} %fusion.8) | copy-start | bytes 2949124
Sparse Core Ops, SparseCore 0:
  145.0 30.2 reduce-scatter.1
where the time goes:
time: 212 us; the launch traced here: 211 us
  waiting for transfers between devices  102 us (48%)
  matrix products  29.2 us (14%)
  starting transfers between devices  27.6 us (13%)
  local copies, waits for them, and re-layouts  22 us (10%)
  between operations  14.2 us (7%)
  blocking collectives  13.3 us (6%)
    all_to_all x1, waiting for transfers between devices, on_device(): lax.all_to_all(send_rows.reshape(experts, capacity, width), 'ep', split_a...  43.1 us
    all_to_all x1, waiting for transfers between devices, on_device(): lax.all_to_all(send_back.reshape(experts, capacity, width), 'ep', split_a...  39 us
    reduce_scatter x1, waiting for transfers between devices, on_device(): lax.psum_scatter(row_part.reshape(experts, capacity, width).astype(jnp.bf...  12.6 us
    all_gather x1, blocking collectives, on_device(): grad_tokens = lax.all_gather(feature_part, 'tp', axis=1, tiled=True)  7.65 us
    all_to_all x1, starting transfers between devices, on_device(): lax.all_to_all(slot_weight.reshape(experts, capacity), 'ep', split_axis=0...  7.28 us
    all_to_all x1, waiting for transfers between devices, on_device(): lax.all_to_all(back_grad, 'ep', split_axis=0, concat_axis=0, tiled=True)  6.41 us
    psum x1, blocking collectives, on_device(): slot_sum = lax.psum(slot_part.astype(jnp.bfloat16), 'tp')  5.65 us
    all_to_all x1, starting transfers between devices, on_device(): lax.all_to_all(send_rows.reshape(experts, capacity, width), 'ep', split_a...  5.54 us
  transfers between devices with their start and end apart: 6, of which 6 were waited for; matrix products, arithmetic and copies ran while one was open for 16% of the time, Pallas kernels for 0%

commit v1 on v0

v1 whole, which is shorter than its diff:
```python
import jax
import jax.numpy as jnp
from jax import lax
from jax.sharding import PartitionSpec as P

BF = jnp.bfloat16
F32 = jnp.float32


def swap(x, mask):
    n = lax.axis_size("tp")
    return lax.ppermute(x, "tp", [(i, i ^ mask) for i in range(n)])


def gather_tp(block):
    n = lax.axis_size("tp")
    blocks = {0: block}
    mask = n // 2
    while mask:
        for d in list(blocks):
            blocks[d ^ mask] = swap(blocks[d], mask)
        mask //= 2
    return [blocks[d] for d in range(n)]


def reorder(x, mask):
    n = lax.axis_size("tp")
    rows = x.shape[0] // n
    return jnp.concatenate([x[(d ^ mask) * rows : ((d ^ mask) + 1) * rows] for d in range(n)], 0)


def on_device(tokens, cotangent, routing, route_weights, w_gate, w_up, w_down):
    experts = lax.axis_size("ep")
    n_tp = lax.axis_size("tp")
    me = lax.axis_index("tp")
    local_tokens, top_count = routing.shape
    width = tokens.shape[1]
    capacity = max(2, (5 * local_tokens * top_count + 4 * experts - 1) // (4 * experts))
    part = -(-capacity // n_tp)
    rows_q = part + 1
    if rows_q > 8:
        rows_q = -(-rows_q // 16) * 16
    spare = rows_q - 1
    block = experts * rows_q
    feat = width // n_tp

    flat = routing.reshape(-1)
    onehot = (flat[:, None] == jnp.arange(experts, dtype=jnp.int32)[None, :]).astype(jnp.int32)
    before = jnp.cumsum(onehot, axis=0) - onehot
    within = jnp.sum(before * onehot, axis=1)
    owner = within // part
    place = flat * rows_q + (within - owner * part)
    owner = owner.reshape(local_tokens, top_count)
    place = place.reshape(local_tokens, top_count)

    ids = jnp.arange(block, dtype=jnp.int32)[:, None, None]

    def picked_of(d):
        here = jnp.where(owner == (me ^ d), place, -1)
        return ids == here[None]

    mine = picked_of(0)
    by_token = jnp.any(mine, axis=2).astype(BF)
    slot_weight = jnp.sum(jnp.where(mine, route_weights[None], 0.0), axis=(1, 2))
    wrow = slot_weight.reshape(experts, rows_q)
    wrow = jnp.pad(wrow, ((0, 0), (0, width - rows_q)))[:, None, :]
    is_spare = (jnp.arange(rows_q) == spare)[None, :, None]
    send_rows = jnp.dot(by_token, tokens, preferred_element_type=F32).reshape(
        experts, rows_q, width
    )
    send_rows = jnp.where(is_spare, wrow, send_rows).astype(BF)
    send_back = jnp.dot(by_token, cotangent, preferred_element_type=F32).astype(BF)
    send_back = send_back.reshape(experts, rows_q, width)

    rows_in = lax.all_to_all(send_rows, "ep", split_axis=0, concat_axis=0, tiled=True)
    back_in = lax.all_to_all(send_back, "ep", split_axis=0, concat_axis=0, tiled=True)
    rows = jnp.concatenate(gather_tp(rows_in.reshape(block, width)), 0)
    back = jnp.concatenate(gather_tp(back_in.reshape(block, width)), 0)
    slots = n_tp * block
    weight = rows.reshape(n_tp * experts, rows_q, width)[:, spare, :rows_q]
    weight = weight.reshape(slots, 1).astype(F32)

    wgate = w_gate[0]
    wup = w_up[0]
    wdown = w_down[0]
    pre_gate = jnp.dot(rows, wgate, preferred_element_type=F32)
    pre_up = jnp.dot(rows, wup, preferred_element_type=F32)
    along = jnp.einsum("rd,fd->rf", back, wdown, preferred_element_type=F32)
    gate_sig = jax.nn.sigmoid(pre_gate)
    gate_act = pre_gate * gate_sig
    hidden = gate_act * pre_up
    hidden_grad = weight * along
    gate_grad = (hidden_grad * pre_up * gate_sig * (1.0 + pre_gate * (1.0 - gate_sig))).astype(BF)
    up_grad = (hidden_grad * gate_act).astype(BF)
    scaled = (weight * hidden).astype(BF)
    slot_part = jnp.sum(hidden * along, axis=1).astype(BF).astype(F32)
    srow = slot_part.reshape(n_tp * experts, rows_q)
    srow = jnp.pad(srow, ((0, 0), (0, feat - rows_q)))[:, None, :]

    def row_part(d):
        at = (me ^ d) * feat
        wg = lax.dynamic_slice_in_dim(wgate, at, feat, 0)
        wu = lax.dynamic_slice_in_dim(wup, at, feat, 0)
        out = jnp.einsum("rf,df->rd", gate_grad, wg, preferred_element_type=F32)
        out = out + jnp.einsum("rf,df->rd", up_grad, wu, preferred_element_type=F32)
        out = jnp.where(is_spare, srow, out.reshape(n_tp * experts, rows_q, feat))
        return out.astype(BF).reshape(slots, feat)

    order = sorted(range(n_tp), key=lambda d: -(d & 1) * n_tp - d)
    parts = {d: row_part(d) for d in order}
    mask = 1
    while mask < n_tp:
        for d in [d for d in sorted(parts, reverse=True) if d & mask]:
            got = reorder(swap(parts.pop(d), mask), mask)
            parts[d ^ mask] = (parts[d ^ mask].astype(F32) + got.astype(F32)).astype(BF)
        mask *= 2
    share = parts[0].reshape(n_tp, experts, rows_q, feat)
    home = lax.all_to_all(share, "ep", split_axis=1, concat_axis=1, tiled=True)

    grad_gate = jnp.einsum("rd,rf->df", rows, gate_grad, preferred_element_type=F32).astype(BF)
    grad_up = jnp.einsum("rd,rf->df", rows, up_grad, preferred_element_type=F32).astype(BF)
    grad_down = jnp.einsum("rf,rd->fd", scaled, back, preferred_element_type=F32).astype(BF)

    pick_home = jnp.concatenate([picked_of(d) for d in range(n_tp)], 0)
    home_by = jnp.any(pick_home, axis=2).astype(BF)
    feature_part = jnp.einsum(
        "st,sd->td", home_by, home.reshape(slots, feat), preferred_element_type=F32
    ).astype(BF)
    slot_grad = home[:, :, spare, :rows_q].reshape(slots, 1, 1).astype(F32)
    grad_weights = jnp.sum(jnp.where(pick_home, slot_grad, 0.0), axis=0).astype(BF)
    grad_tokens = lax.all_gather(feature_part, "tp", axis=1, tiled=True)
    return (grad_tokens, grad_weights, grad_gate[None], grad_up[None], grad_down[None])


def solution(mesh):
    row = P("ep", None)
    col = P("ep", None, "tp")
    low = P("ep", "tp", None)
    return jax.shard_map(
        on_device,
        mesh=mesh,
        in_specs=(row, row, row, row, col, col, low),
        out_specs=(row, row, col, col, low),
        check_vma=False,
    )
```

time: 212 us -> 125 us (0.59)
  waiting for transfers between devices: 102 us -> 50.9 us
  local copies, waits for them, and re-layouts: 22 us -> 5.26 us
  between operations: 14.2 us -> 1.04 us
  starting transfers between devices: 27.6 us -> 21.8 us
  blocking collectives: 13.3 us -> 8.63 us
  other arithmetic: 2.02 us -> 6.12 us
    all_to_all x5 -> x3, waiting for transfers between devices: 89.9 us -> 32.4 us  [the longest x1 13.3 us: on_device(): lax.all_to_all(send_rows, 'ep', split_axis=0, concat_axis=0, tiled=True)]
    ppermute x0 -> x9, waiting for transfers between devices: none -> 18.4 us  [swap(): return lax.ppermute(x, 'tp', [(i, i ^ mask) for i in range(n)])]
    reduce_scatter x1 -> x0, waiting for transfers between devices: 12.6 us -> none  [on_device(): lax.psum_scatter(row_part.reshape(experts, capacity, width).astype(jnp.bf...]
    all_to_all x5 -> x3, starting transfers between devices: 27.5 us -> 16 us  [the longest x1 7.28 us: on_device(): lax.all_to_all(send_rows, 'ep', split_axis=0, concat_axis=0, tiled=True)]
    reshape x7 -> x2, local copies, waits for them, and re-layouts: 11.1 us -> 0.91 us  [the longest x1 0.82 us: on_device(): share = parts[0].reshape(n_tp, experts, rows_q, feat)]
    ppermute x0 -> x9, starting transfers between devices: none -> 5.86 us  [swap(): return lax.ppermute(x, 'tp', [(i, i ^ mask) for i in range(n)])]
    psum x1 -> x0, blocking collectives: 5.65 us -> none  [on_device(): slot_sum = lax.psum(slot_part.astype(jnp.bfloat16), 'tp')]
    convert_element_type x3, local copies, waits for them, and re-layouts: 3.46 us -> 0.24 us  [the longest x1 0.09 us: on_device(): slot_part = jnp.sum(hidden * along, axis=1).astype(BF).astype(F32)]
  transfers between devices with their start and end apart: 6 -> 12, of which waited for: 6 -> 5; matrix products, arithmetic and copies ran while one was open for 16% -> 20% of each run, Pallas kernels for 0% -> 0%
where the time goes in v1:
time: 125 us; the launch traced here: 124 us
  waiting for transfers between devices  50.9 us (41%)
  matrix products  30.5 us (24%)
  starting transfers between devices  21.8 us (17%)
  blocking collectives  8.63 us (7%)
  other arithmetic  6.12 us (5%)
  local copies, waits for them, and re-layouts  5.26 us (4%)
    ppermute x9, waiting for transfers between devices, swap(): return lax.ppermute(x, 'tp', [(i, i ^ mask) for i in range(n)])  18.4 us
    all_to_all x1, waiting for transfers between devices, on_device(): lax.all_to_all(send_rows, 'ep', split_axis=0, concat_axis=0, tiled=True)  13.3 us
    all_to_all x1, waiting for transfers between devices, on_device(): lax.all_to_all(send_back, 'ep', split_axis=0, concat_axis=0, tiled=True)  13.1 us
    all_gather x1, blocking collectives, on_device(): grad_tokens = lax.all_gather(feature_part, 'tp', axis=1, tiled=True)  8.63 us
    all_to_all x1, starting transfers between devices, on_device(): lax.all_to_all(send_rows, 'ep', split_axis=0, concat_axis=0, tiled=True)  7.28 us
    all_to_all x1, waiting for transfers between devices, on_device(): home = lax.all_to_all(share, 'ep', split_axis=1, concat_axis=1, tiled=True)  5.96 us
    ppermute x9, starting transfers between devices, swap(): return lax.ppermute(x, 'tp', [(i, i ^ mask) for i in range(n)])  5.86 us
    all_to_all x1, starting transfers between devices, on_device(): home = lax.all_to_all(share, 'ep', split_axis=1, concat_axis=1, tiled=True)  5.06 us
  transfers between devices with their start and end apart: 12, of which 5 were waited for; matrix products, arithmetic and copies ran while one was open for 20% of the time, Pallas kernels for 0%

profile of v1, /device:TPU:0, one launch (start us, length us, event | category | flops | bytes accessed | tf_op | source)
XLA Modules:
  0.0 124.3 jit_solution(13464868336835828591)
XLA Ops:
  0.7 1.0 copy.71
  1.9 0.9 reduce-window.6
  3.4 0.7 compare_select_fusion.3
  4.1 0.9 select_reduce_fusion.1
  5.1 0.7 compare_select_fusion.2
  6.1 2.2 %fusion.3 = bf16[8,16,2048]{2,1,0:T(8,128)(2,1)} fusion(pred[8,16,192]{2,1,0:T(8,128)(4,1)S(1)} %bitcast.118, bf16[192,2048]{1,0:T(8,128)(2,1)} %param.7, bf16[8,2048]{1,0:T(8,128)(2,1)S(1)} %pad.11, pred[16]{0:T(512)(128)(4,1)S(1)} %iota_compare_fusion.6), kind=kOutput, calls=%fused_computation.11 | convolution fusion | flops 100925440 | bytes 1368080 | tf_op jit(solution)/shard_map/dot_general | solution.py:68
  8.3 7.3 %all-to-all-start = ((bf16[8,16,2048]{2,1,0:T(8,128)(2,1)}), bf16[8,16,2048]{2,1,0:T(8,128)(2,1)S(1)}, u32[]{:S(2)}, u32[]{:S(2)}) async-start(bf16[8,16,2048]{2,1,0:T(8,128)(2,1)} %fusion.3), calls=%async_computation | async-start | bytes 1048576 | tf_op jit(solution)/shard_map/all_to_all | solution.py:75
  15.6 1.1 convolution_convert_fusion.3
  16.7 13.3 %all-to-all-done = bf16[8,16,2048]{2,1,0:T(8,128)(2,1)S(1)} async-done(((bf16[8,16,2048]{2,1,0:T(8,128)(2,1)}), bf16[8,16,2048]{2,1,0:T(8,128)(2,1)S(1)}, u32[]{:S(2)}, u32[]{:S(2)}) %all-to-all-start) | async-done | bytes 524320 | tf_op jit(solution)/shard_map/all_to_all | solution.py:75
  30.1 3.6 %all-to-all-start.1 = ((bf16[8,16,2048]{2,1,0:T(8,128)(2,1)}), bf16[8,16,2048]{2,1,0:T(8,128)(2,1)S(1)}, u32[]{:S(2)}, u32[]{:S(2)}) async-start(bf16[8,16,2048]{2,1,0:T(8,128)(2,1)} %bitcast.7), calls=%async_computation.1 | async-start | bytes 1048576 | tf_op jit(solution)/shard_map/all_to_all | solution.py:76
  33.7 1.5 %collective-permute-start.1 = (bf16[128,2048]{1,0:T(8,128)(2,1)S(1)}, bf16[128,2048]{1,0:T(8,128)(2,1)}, u32[]{:S(2)}, u32[]{:S(2)}) collective-permute-start(bf16[128,2048]{1,0:T(8,128)(2,1)S(1)} %bitcast.107), channel_id=1, source_target_pairs={{0,2},{1,3},{2,0},{3,1},{4,6},{5,7},{6,4},{7,5},{8,10},{9,11},{10,... | collective-permute-start | bytes 1572872 | tf_op jit(solution)/shard_map/ppermute | solution.py:12
  35.2 13.1 %all-to-all-done.1 = bf16[8,16,2048]{2,1,0:T(8,128)(2,1)S(1)} async-done(((bf16[8,16,2048]{2,1,0:T(8,128)(2,1)}), bf16[8,16,2048]{2,1,0:T(8,128)(2,1)S(1)}, u32[]{:S(2)}, u32[]{:S(2)}) %all-to-all-start.1) | async-done | bytes 524320 | tf_op jit(solution)/shard_map/all_to_all | solution.py:76
  48.4 1.5 %collective-permute-start.4 = (bf16[128,2048]{1,0:T(8,128)(2,1)S(1)}, bf16[128,2048]{1,0:T(8,128)(2,1)}, u32[]{:S(2)}, u32[]{:S(2)}) collective-permute-start(bf16[128,2048]{1,0:T(8,128)(2,1)S(1)} %bitcast.114), channel_id=1, source_target_pairs={{0,2},{1,3},{2,0},{3,1},{4,6},{5,7},{6,4},{7,5},{8,10},{9,11},{10,... | collective-permute-start | bytes 1572872 | tf_op jit(solution)/shard_map/ppermute | solution.py:12
  50.8 10.1 %collective-permute-done.4 = bf16[128,2048]{1,0:T(8,128)(2,1)} collective-permute-done((bf16[128,2048]{1,0:T(8,128)(2,1)S(1)}, bf16[128,2048]{1,0:T(8,128)(2,1)}, u32[]{:S(2)}, u32[]{:S(2)}) %collective-permute-start.4) | collective-permute-done | bytes 524320 | tf_op jit(solution)/shard_map/ppermute | solution.py:12
  60.9 1.6 %pad_maximum_fusion = bf16[512,2048]{1,0:T(8,128)(2,1)S(1)} fusion(bf16[128,2048]{1,0:T(8,128)(2,1)} %collective-permute-done.2, bf16[128,2048]{1,0:T(8,128)(2,1)} %collective-permute-done.1, bf16[128,2048]{1,0:T(8,128)(2,1)} %collective-permute-done, bf16[128,2048]{1,0:T(8,128)(2,1)S(1)} %bitcast.109), kind=kLoop, calls=%fused_computation.13 | loop fusion | flops 8388608 | bytes 4194304 | tf_op jit(solution)/shard_map/concatenate | solution.py:77
  62.5 3.6 %fusion.8 = f32[512,512]{0,1:T(8,128)} fusion(bf16[1,2048,512]{2,1,0:T(8,128)(2,1)S(1)} %copy-done, bf16[128,2048]{1,0:T(8,128)(2,1)} %collective-permute-done.2, bf16[128,2048]{1,0:T(8,128)(2,1)} %collective-permute-done.1, bf16[128,2048]{1,0:T(8,128)(2,1)} %collective-permute-done, bf16[128,2048]{1,0:T(8,128)(2,1)S(1)} %bitcast.110), kind=kOutput, calls=%fused_computation.19 | convolution fusion | flops 1082130432 | bytes 5242880 | tf_op jit(solution)/shard_map/dot_general | solution.py:86
  66.3 3.5 %fusion.6 = f32[512,512]{0,1:T(8,128)S(1)} fusion(bf16[1,2048,512]{2,1,0:T(8,128)(2,1)} %param.12, bf16[128,2048]{1,0:T(8,128)(2,1)} %collective-permute-done.2, bf16[128,2048]{1,0:T(8,128)(2,1)} %collective-permute-done.1, bf16[128,2048]{1,0:T(8,128)(2,1)} %collective-permute-done, bf16[128,2048]{1,0:T(8,128)(2,1)S(1)} %bitcast.111), kind=kOutput, calls=%fused_computation.17 | convolution fusion | flops 1082130432 | bytes 5242880 | tf_op jit(solution)/shard_map/dot_general | solution.py:87
  69.9 3.4 %multiply_reduce_fusion = (bf16[512]{0:T(512)(128)(2,1)S(1)}, bf16[512,512]{0,1:T(8,128)(2,1)S(1)}, bf16[512,512]{0,1:T(8,128)(2,1)S(1)}) fusion(f32[512,512]{0,1:T(8,128)S(1)} %fusion.6, f32[512,512]{0,1:T(8,128)S(1)} %copy-done.9, f32[512]{0:T(512)S(1)} %reshape.121, bf16[1,512,2048]{2,1,0:T(8,128)(2,1)S(1)} %copy-done.8, ...), kind=kOutput, calls=%fused_computation.38 | convolution fusion | flops 1086586368 | bytes 7343104 | tf_op jit(solution)/shard_map/rd,fd->rf/dot_general | solution.py:88
  73.9 1.1 copy-done.1
  75.5 0.6 collective-permute-start.7
  78.2 1.6 %collective-permute-start.8 = (bf16[512,512]{1,0:T(8,128)(2,1)S(1)}, bf16[512,512]{1,0:T(8,128)(2,1)S(1)}, u32[]{:S(2)}, u32[]{:S(2)}) collective-permute-start(bf16[512,512]{1,0:T(8,128)(2,1)S(1)} %add_convert_fusion.1), channel_id=1, source_target_pairs={{0,2},{1,3},{2,0},{3,1},{4,6},{5,7},{6,4},{7,5},{8,10},{9,11},{10,... | collective-permute-start | bytes 1572872 | tf_op jit(solution)/shard_map/ppermute | solution.py:12
  79.8 4.0 %fusion.1 = bf16[1,2048,512]{2,1,0:T(8,128)(2,1)} fusion(bf16[512,512]{0,1:T(8,128)(2,1)S(1)} %get-tuple-element.11, bf16[128,2048]{1,0:T(8,128)(2,1)} %collective-permute-done.2, bf16[128,2048]{1,0:T(8,128)(2,1)} %collective-permute-done.1, bf16[128,2048]{1,0:T(8,128)(2,1)} %collective-permute-done, bf16[128,2048]{1,0:T(8,128)(2,1)S(1)} %bitcast.113), kind=kOutput, calls=%fused_computation.4 | convolution fusion | flops 1083179008 | bytes 4718592 | tf_op jit(solution)/shard_map/rd,rf->df/dot_general | solution.py:121
  84.3 8.3 %collective-permute-done.8 = bf16[512,512]{1,0:T(8,128)(2,1)S(1)} collective-permute-done((bf16[512,512]{1,0:T(8,128)(2,1)S(1)}, bf16[512,512]{1,0:T(8,128)(2,1)S(1)}, u32[]{:S(2)}, u32[]{:S(2)}) %collective-permute-start.8) | collective-permute-done | bytes 524320 | tf_op jit(solution)/shard_map/ppermute | solution.py:12
  92.6 0.6 add_convert_fusion
  93.3 0.8 copy.78
  94.1 5.1 %all-to-all-start.2 = ((bf16[4,8,16,512]{3,2,0,1:T(8,128)(2,1)}), bf16[4,8,16,512]{3,2,0,1:T(8,128)(2,1)S(1)}, u32[]{:S(2)}, u32[]{:S(2)}) async-start(bf16[4,8,16,512]{3,2,0,1:T(8,128)(2,1)} %copy.78), calls=%async_computation.2 | async-start | bytes 1048576 | tf_op jit(solution)/shard_map/all_to_all | solution.py:118
  99.2 4.3 %fusion = bf16[1,2048,512]{2,1,0:T(8,128)(2,1)} fusion(bf16[512,512]{0,1:T(8,128)(2,1)S(1)} %get-tuple-element.10, bf16[128,2048]{1,0:T(8,128)(2,1)} %collective-permute-done.2, bf16[128,2048]{1,0:T(8,128)(2,1)} %collective-permute-done.1, bf16[128,2048]{1,0:T(8,128)(2,1)} %collective-permute-done, bf16[128,2048]{1,0:T(8,128)(2,1)} %bitcast.112), kind=kOutput, calls=%fused_computation.3 | convolution fusion | flops 1083179008 | bytes 4718592 | tf_op jit(solution)/shard_map/rd,rf->df/dot_general | solution.py:120
  103.5 4.0 %fusion.2 = bf16[1,512,2048]{2,1,0:T(8,128)(2,1)} fusion(f32[512]{0:T(512)S(1)} %reshape.121, f32[512,512]{0,1:T(8,128)S(1)} %copy-done.12, bf16[128,2048]{1,0:T(8,128)(2,1)} %collective-permute-done.5, bf16[128,2048]{1,0:T(8,128)(2,1)} %collective-permute-done.4, bf16[128,2048]{1,0:T(8,128)(2,1)} %collective-permute-done.3, ...), kind=kOutput, calls=%fused_computation.5 | convolution fusion | flops 1085014016 | bytes 6293504 | tf_op jit(solution)/shard_map/rf,rd->fd/dot_general | solution.py:122
  107.5 6.0 %all-to-all-done.2 = bf16[4,8,16,512]{3,2,0,1:T(8,128)(2,1)S(1)} async-done(((bf16[4,8,16,512]{3,2,0,1:T(8,128)(2,1)}), bf16[4,8,16,512]{3,2,0,1:T(8,128)(2,1)S(1)}, u32[]{:S(2)}, u32[]{:S(2)}) %all-to-all-start.2) | async-done | bytes 524320 | tf_op jit(solution)/shard_map/all_to_all | solution.py:118
  113.6 0.8 select_reduce_fusion
  114.8 8.6 %all_gather.3 = bf16[192,2048]{1,0:T(8,128)(2,1)S(1)} all-gather(bf16[192,512]{1,0:T(8,128)(2,1)S(1)} %convolution_convert_fusion.4), channel_id=1, replica_groups=mesh['ep'=8,'tp'=4] {'tp'}, dimensions={1}, use_global_device_ids=true | all-gather | bytes 983040 | tf_op jit(solution)/shard_map/all_gather | solution.py:131
  123.4 0.9 copy.84
  (73 shorter events, 6.5 us)
Async XLA Ops:
  0.6 61.9 %copy-start = (bf16[1,2048,512]{2,1,0:T(8,128)(2,1)S(1)}, bf16[1,2048,512]{2,1,0:T(8,128)(2,1)}, u32[]{:S(2)}) copy-start(bf16[1,2048,512]{2,1,0:T(8,128)(2,1)} %param.11) | copy-start | bytes 6291460
  0.6 14.9 %copy-start.4 = (bf16[192,2048]{1,0:T(8,128)(2,1)S(1)}, bf16[192,2048]{1,0:T(8,128)(2,1)}, u32[]{:S(2)}) copy-start(bf16[192,2048]{1,0:T(8,128)(2,1)} %param.8) | copy-start | bytes 2359300
  8.3 21.8 %all-to-all-start = ((bf16[8,16,2048]{2,1,0:T(8,128)(2,1)}), bf16[8,16,2048]{2,1,0:T(8,128)(2,1)S(1)}, u32[]{:S(2)}, u32[]{:S(2)}) async-start(bf16[8,16,2048]{2,1,0:T(8,128)(2,1)} %fusion.3), calls=%async_computation | async-start | bytes 1048576 | tf_op jit(solution)/shard_map/all_to_all | solution.py:75
  30.1 36.2 %copy-start.2 = (bf16[8,16,2048]{2,1,0:T(8,128)(2,1)}, bf16[8,16,2048]{2,1,0:T(8,128)(2,1)S(1)}, u32[]{:S(2)}) copy-start(bf16[8,16,2048]{2,1,0:T(8,128)(2,1)S(1)} %all-to-all-done) | copy-start | bytes 1572868
  30.1 18.3 %all-to-all-start.1 = ((bf16[8,16,2048]{2,1,0:T(8,128)(2,1)}), bf16[8,16,2048]{2,1,0:T(8,128)(2,1)S(1)}, u32[]{:S(2)}, u32[]{:S(2)}) async-start(bf16[8,16,2048]{2,1,0:T(8,128)(2,1)} %bitcast.7), calls=%async_computation.1 | async-start | bytes 1048576 | tf_op jit(solution)/shard_map/all_to_all | solution.py:76
  33.7 16.2 %collective-permute-start.1 = (bf16[128,2048]{1,0:T(8,128)(2,1)S(1)}, bf16[128,2048]{1,0:T(8,128)(2,1)}, u32[]{:S(2)}, u32[]{:S(2)}) collective-permute-start(bf16[128,2048]{1,0:T(8,128)(2,1)S(1)} %bitcast.107), channel_id=1, source_target_pairs={{0,2},{1,3},{2,0},{3,1},{4,6},{5,7},{6,4},{7,5},{8,10},{9,11},{10,... | collective-permute-start | bytes 1572872 | tf_op jit(solution)/shard_map/ppermute | solution.py:12
  48.4 14.1 %copy-start.5 = (bf16[8,16,2048]{2,1,0:T(8,128)(2,1)}, bf16[8,16,2048]{2,1,0:T(8,128)(2,1)S(1)}, u32[]{:S(2)}) copy-start(bf16[8,16,2048]{2,1,0:T(8,128)(2,1)S(1)} %all-to-all-done.1) | copy-start | bytes 1572868
  48.4 12.5 %collective-permute-start.4 = (bf16[128,2048]{1,0:T(8,128)(2,1)S(1)}, bf16[128,2048]{1,0:T(8,128)(2,1)}, u32[]{:S(2)}, u32[]{:S(2)}) collective-permute-start(bf16[128,2048]{1,0:T(8,128)(2,1)S(1)} %bitcast.114), channel_id=1, source_target_pairs={{0,2},{1,3},{2,0},{3,1},{4,6},{5,7},{6,4},{7,5},{8,10},{9,11},{10,... | collective-permute-start | bytes 1572872 | tf_op jit(solution)/shard_map/ppermute | solution.py:12
  49.9 11.0 %collective-permute-start = (bf16[128,2048]{1,0:T(8,128)(2,1)S(1)}, bf16[128,2048]{1,0:T(8,128)(2,1)}, u32[]{:S(2)}, u32[]{:S(2)}) collective-permute-start(bf16[128,2048]{1,0:T(8,128)(2,1)S(1)} %bitcast.108), channel_id=1, source_target_pairs={{0,1},{1,0},{2,3},{3,2},{4,5},{5,4},{6,7},{7,6},{8,9},{9,8},{10,11... | collective-permute-start | bytes 1572872 | tf_op jit(solution)/shard_map/ppermute | solution.py:12
  49.9 11.0 %collective-permute-start.2 = (bf16[128,2048]{1,0:T(8,128)(2,1)}, bf16[128,2048]{1,0:T(8,128)(2,1)}, u32[]{:S(2)}, u32[]{:S(2)}) collective-permute-start(bf16[128,2048]{1,0:T(8,128)(2,1)} %collective-permute-done.1), channel_id=1, source_target_pairs={{0,1},{1,0},{2,3},{3,2},{4,5},{5,4},{6,7},{7,6},{8,9},{9,8},{10,11... | collective-permute-start | bytes 1572872 | tf_op jit(solution)/shard_map/ppermute | solution.py:12
  50.7 19.2 %collective-permute-start.3 = (bf16[128,2048]{1,0:T(8,128)(2,1)S(1)}, bf16[128,2048]{1,0:T(8,128)(2,1)}, u32[]{:S(2)}, u32[]{:S(2)}) collective-permute-start(bf16[128,2048]{1,0:T(8,128)(2,1)S(1)} %bitcast.115), channel_id=1, source_target_pairs={{0,1},{1,0},{2,3},{3,2},{4,5},{5,4},{6,7},{7,6},{8,9},{9,8},{10,11... | collective-permute-start | bytes 1572872 | tf_op jit(solution)/shard_map/ppermute | solution.py:12
  60.9 9.0 %collective-permute-start.5 = (bf16[128,2048]{1,0:T(8,128)(2,1)}, bf16[128,2048]{1,0:T(8,128)(2,1)}, u32[]{:S(2)}, u32[]{:S(2)}) collective-permute-start(bf16[128,2048]{1,0:T(8,128)(2,1)} %collective-permute-done.4), channel_id=1, source_target_pairs={{0,1},{1,0},{2,3},{3,2},{4,5},{5,4},{6,7},{7,6},{8,9},{9,8},{10,11... | collective-permute-start | bytes 1572872 | tf_op jit(solution)/shard_map/ppermute | solution.py:12
  66.3 3.6 %copy-start.6 = (bf16[8,16,2048]{2,1,0:T(8,128)(2,1)S(1)}, bf16[8,16,2048]{2,1,0:T(8,128)(2,1)}, u32[]{:S(2)}) copy-start(bf16[8,16,2048]{2,1,0:T(8,128)(2,1)} %copy-done.5) | copy-start | bytes 1572868
  66.3 3.6 %copy-start.8 = (bf16[1,512,2048]{2,1,0:T(8,128)(2,1)S(1)}, bf16[1,512,2048]{2,1,0:T(8,128)(2,1)}, u32[]{:S(2)}) copy-start(bf16[1,512,2048]{2,1,0:T(8,128)(2,1)} %param.13) | copy-start | bytes 6291460
  66.3 3.6 %copy-start.9 = (f32[512,512]{0,1:T(8,128)S(1)}, f32[512,512]{0,1:T(8,128)}, u32[]{:S(2)}) copy-start(f32[512,512]{0,1:T(8,128)} %fusion.8) | copy-start | bytes 3145732
  69.8 3.5 %copy-start.11 = (f32[512,512]{0,1:T(8,128)}, f32[512,512]{0,1:T(8,128)S(1)}, u32[]{:S(2)}) copy-start(f32[512,512]{0,1:T(8,128)S(1)} %fusion.6) | copy-start | bytes 3145732
  73.4 1.6 %copy-start.1 = (bf16[1,2048,512]{2,1,0:T(8,128)(2,1)S(1)}, bf16[1,2048,512]{2,1,0:T(8,128)(2,1)}, u32[]{:S(2)}) copy-start(bf16[1,2048,512]{2,1,0:T(8,128)(2,1)} %param.12) | copy-start | bytes 6291460
  75.5 2.1 %collective-permute-start.7 = (bf16[512,512]{1,0:T(8,128)(2,1)S(1)}, bf16[512,512]{1,0:T(8,128)(2,1)S(1)}, u32[]{:S(2)}, u32[]{:S(2)}) collective-permute-start(bf16[512,512]{1,0:T(8,128)(2,1)S(1)} %fusion.15), channel_id=1, source_target_pairs={{0,1},{1,0},{2,3},{3,2},{4,5},{5,4},{6,7},{7,6},{8,9},{9,8},{10,11... | collective-permute-start | bytes 1572872 | tf_op jit(solution)/shard_map/ppermute | solution.py:12
  77.0 7.3 %collective-permute-start.6 = (bf16[512,512]{1,0:T(8,128)(2,1)S(1)}, bf16[512,512]{1,0:T(8,128)(2,1)S(1)}, u32[]{:S(2)}, u32[]{:S(2)}) collective-permute-start(bf16[512,512]{1,0:T(8,128)(2,1)S(1)} %fusion.12), channel_id=1, source_target_pairs={{0,1},{1,0},{2,3},{3,2},{4,5},{5,4},{6,7},{7,6},{8,9},{9,8},{10,11... | collective-permute-start | bytes 1572872 | tf_op jit(solution)/shard_map/ppermute | solution.py:12
  77.6 2.2 %copy-start.3 = (bf16[8,16,2048]{2,1,0:T(8,128)(2,1)S(1)}, bf16[8,16,2048]{2,1,0:T(8,128)(2,1)}, u32[]{:S(2)}) copy-start(bf16[8,16,2048]{2,1,0:T(8,128)(2,1)} %copy-done.2) | copy-start | bytes 1572868
  78.2 14.4 %collective-permute-start.8 = (bf16[512,512]{1,0:T(8,128)(2,1)S(1)}, bf16[512,512]{1,0:T(8,128)(2,1)S(1)}, u32[]{:S(2)}, u32[]{:S(2)}) collective-permute-start(bf16[512,512]{1,0:T(8,128)(2,1)S(1)} %add_convert_fusion.1), channel_id=1, source_target_pairs={{0,2},{1,3},{2,0},{3,1},{4,6},{5,7},{6,4},{7,5},{8,10},{9,11},{10,... | collective-permute-start | bytes 1572872 | tf_op jit(solution)/shard_map/ppermute | solution.py:12
  94.1 19.3 %all-to-all-start.2 = ((bf16[4,8,16,512]{3,2,0,1:T(8,128)(2,1)}), bf16[4,8,16,512]{3,2,0,1:T(8,128)(2,1)S(1)}, u32[]{:S(2)}, u32[]{:S(2)}) async-start(bf16[4,8,16,512]{3,2,0,1:T(8,128)(2,1)} %copy.78), calls=%async_computation.2 | async-start | bytes 1048576 | tf_op jit(solution)/shard_map/all_to_all | solution.py:118
  99.2 4.3 %copy-start.7 = (bf16[8,16,2048]{2,1,0:T(8,128)(2,1)S(1)}, bf16[8,16,2048]{2,1,0:T(8,128)(2,1)}, u32[]{:S(2)}) copy-start(bf16[8,16,2048]{2,1,0:T(8,128)(2,1)} %copy-done.5) | copy-start | bytes 1572868
  99.2 4.3 %copy-start.10 = (f32[512,512]{0,1:T(8,128)S(1)}, f32[512,512]{0,1:T(8,128)}, u32[]{:S(2)}) copy-start(f32[512,512]{0,1:T(8,128)} %fusion.8) | copy-start | bytes 3145732
  99.2 4.3 %copy-start.12 = (f32[512,512]{0,1:T(8,128)S(1)}, f32[512,512]{0,1:T(8,128)}, u32[]{:S(2)}) copy-start(f32[512,512]{0,1:T(8,128)} %copy-done.11) | copy-start | bytes 3145732

commit v2 on v1

--- a/solution.py
+++ b/solution.py
@@ -1,6 +1,8 @@
 import jax
 import jax.numpy as jnp
 from jax import lax
+from jax.experimental import pallas as pl
+from jax.experimental.pallas import tpu as pltpu
 from jax.sharding import PartitionSpec as P
 
 BF = jnp.bfloat16
@@ -12,13 +14,16 @@
     return lax.ppermute(x, "tp", [(i, i ^ mask) for i in range(n)])
 
 
-def gather_tp(block):
+def gather_tp(block, hold=None):
     n = lax.axis_size("tp")
     blocks = {0: block}
     mask = n // 2
     while mask:
         for d in list(blocks):
-            blocks[d ^ mask] = swap(blocks[d], mask)
+            sent = blocks[d]
+            if hold is not None and mask == 1 and d in (0, n // 2):
+                sent = hold(sent, d)
+            blocks[d ^ mask] = swap(sent, mask)
         mask //= 2
     return [blocks[d] for d in range(n)]
 
@@ -27,6 +32,58 @@
     n = lax.axis_size("tp")
     rows = x.shape[0] // n
     return jnp.concatenate([x[(d ^ mask) * rows : ((d ^ mask) + 1) * rows] for d in range(n)], 0)
+
+
+def dispatch(me, routing, route_weights, tokens, cotangent, experts, part, rows_q):
+    count, width = tokens.shape
+    top_count = routing.shape[0]
+    block = experts * rows_q
+
+    def body(me_ref, route_ref, weight_ref, tok_ref, cot_ref, rows_ref, back_ref, within_ref):
+        expert = lax.broadcasted_iota(jnp.int32, (experts, count), 0)
+        names = [route_ref[k : k + 1, :] for k in range(top_count)]
+        named = sum((name == expert).astype(F32) for name in names).astype(BF)
+        earlier = lax.broadcasted_iota(jnp.int32, (count, count), 0) < lax.broadcasted_iota(
+            jnp.int32, (count, count), 1
+        )
+        before = jnp.dot(named, earlier.astype(F32).astype(BF), preferred_element_type=F32)
+        slot = lax.broadcasted_iota(jnp.int32, (block, count), 0)
+        near = lax.broadcasted_iota(jnp.int32, (128, count), 0)
+        picked = jnp.zeros((block, count), F32)
+        spares = jnp.zeros((block, 128), F32)
+        for k, name in enumerate(names):
+            within = jnp.sum(jnp.where(name == expert, before, 0.0), axis=0, keepdims=True)
+            within = within.astype(jnp.int32)
+            within_ref[k : k + 1, :] = within
+            local = within - me_ref[0] * part
+            mine = (local >= 0) & (local < part)
+            at = jnp.where(mine, name * rows_q + local, -1)
+            picked = picked + (slot == at).astype(F32)
+            row = jnp.where(mine, name * rows_q + rows_q - 1, -1)
+            weight = jnp.where(near == local, weight_ref[k : k + 1, :], 0.0).astype(BF)
+            spares = spares + lax.dot_general(
+                (slot == row).astype(F32).astype(BF), weight, (((1,), (1,)), ((), ())),
+                preferred_element_type=F32,
+            )
+        picked = picked.astype(BF)
+        sent = jnp.dot(picked, tok_ref[...], preferred_element_type=F32)
+        rows_ref[...] = sent.astype(BF)
+        rows_ref[:, 0:128] = (sent[:, 0:128] + spares).astype(BF)
+        sent = jnp.dot(picked, cot_ref[...], preferred_element_type=F32)
+        back_ref[...] = sent.astype(BF)
+
+    vmem = pl.BlockSpec(memory_space=pltpu.VMEM)
+    return pl.pallas_call(
+        body,
+        name="dispatch",
+        in_specs=[pl.BlockSpec(memory_space=pltpu.SMEM)] + [vmem] * 4,
+        out_specs=[vmem] * 3,
+        out_shape=[
+            jax.ShapeDtypeStruct((block, width), BF),
+            jax.ShapeDtypeStruct((block, width), BF),
+            jax.ShapeDtypeStruct((top_count, count), jnp.int32),
+        ],
+    )(me.reshape(1).astype(jnp.int32), routing, route_weights, tokens, cotangent)
 
 
 def on_device(tokens, cotangent, routing, route_weights, w_gate, w_up, w_down):
@@ -44,47 +101,36 @@
     block = experts * rows_q
     feat = width // n_tp
 
-    flat = routing.reshape(-1)
-    onehot = (flat[:, None] == jnp.arange(experts, dtype=jnp.int32)[None, :]).astype(jnp.int32)
-    before = jnp.cumsum(onehot, axis=0) - onehot
-    within = jnp.sum(before * onehot, axis=1)
-    owner = within // part
-    place = flat * rows_q + (within - owner * part)
-    owner = owner.reshape(local_tokens, top_count)
-    place = place.reshape(local_tokens, top_count)
-
-    ids = jnp.arange(block, dtype=jnp.int32)[:, None, None]
-
-    def picked_of(d):
-        here = jnp.where(owner == (me ^ d), place, -1)
-        return ids == here[None]
-
-    mine = picked_of(0)
-    by_token = jnp.any(mine, axis=2).astype(BF)
-    slot_weight = jnp.sum(jnp.where(mine, route_weights[None], 0.0), axis=(1, 2))
-    wrow = slot_weight.reshape(experts, rows_q)
-    wrow = jnp.pad(wrow, ((0, 0), (0, width - rows_q)))[:, None, :]
+    routing = routing.T
+    send_rows, send_back, within = dispatch(
+        me, routing, route_weights.T, tokens, cotangent, experts, part, rows_q
+    )
+    send_rows = send_rows.reshape(experts, rows_q, width)
+    send_back = send_back.reshape(experts, rows_q, width)
     is_spare = (jnp.arange(rows_q) == spare)[None, :, None]
-    send_rows = jnp.dot(by_token, tokens, preferred_element_type=F32).reshape(
-        experts, rows_q, width
-    )
-    send_rows = jnp.where(is_spare, wrow, send_rows).astype(BF)
-    send_back = jnp.dot(by_token, cotangent, preferred_element_type=F32).astype(BF)
-    send_back = send_back.reshape(experts, rows_q, width)
 
     rows_in = lax.all_to_all(send_rows, "ep", split_axis=0, concat_axis=0, tiled=True)
     back_in = lax.all_to_all(send_back, "ep", split_axis=0, concat_axis=0, tiled=True)
     rows = jnp.concatenate(gather_tp(rows_in.reshape(block, width)), 0)
-    back = jnp.concatenate(gather_tp(back_in.reshape(block, width)), 0)
-    slots = n_tp * block
-    weight = rows.reshape(n_tp * experts, rows_q, width)[:, spare, :rows_q]
-    weight = weight.reshape(slots, 1).astype(F32)
-
     wgate = w_gate[0]
     wup = w_up[0]
     wdown = w_down[0]
     pre_gate = jnp.dot(rows, wgate, preferred_element_type=F32)
     pre_up = jnp.dot(rows, wup, preferred_element_type=F32)
+
+    def hold(blocks, d):
+        nonlocal pre_gate, pre_up
+        if d == 0:
+            blocks, pre_gate = lax.optimization_barrier((blocks, pre_gate))
+        else:
+            blocks, pre_gate, pre_up = lax.optimization_barrier((blocks, pre_gate, pre_up))
+        return blocks
+
+    back = jnp.concatenate(gather_tp(back_in.reshape(block, width), hold), 0)
+    slots = n_tp * block
+    weight = rows.reshape(n_tp * experts, rows_q, width)[:, spare, :rows_q]
+    weight = weight.reshape(slots, 1).astype(F32)
+
     along = jnp.einsum("rd,fd->rf", back, wdown, preferred_element_type=F32)
     gate_sig = jax.nn.sigmoid(pre_gate)
     gate_act = pre_gate * gate_sig
@@ -121,13 +167,23 @@
     grad_up = jnp.einsum("rd,rf->df", rows, up_grad, preferred_element_type=F32).astype(BF)
     grad_down = jnp.einsum("rf,rd->fd", scaled, back, preferred_element_type=F32).astype(BF)
 
-    pick_home = jnp.concatenate([picked_of(d) for d in range(n_tp)], 0)
-    home_by = jnp.any(pick_home, axis=2).astype(BF)
+    owner = within // part
+    within = within - owner * part
+    at_block = (owner ^ me) * experts + routing
+    ids = jnp.arange(slots, dtype=jnp.int32)[:, None]
+    home_at = at_block * rows_q + within
+    home_by = sum((ids == home_at[k : k + 1]).astype(BF) for k in range(top_count))
     feature_part = jnp.einsum(
         "st,sd->td", home_by, home.reshape(slots, feat), preferred_element_type=F32
     ).astype(BF)
-    slot_grad = home[:, :, spare, :rows_q].reshape(slots, 1, 1).astype(F32)
-    grad_weights = jnp.sum(jnp.where(pick_home, slot_grad, 0.0), axis=0).astype(BF)
+    spares = home[:, :, spare, :rows_q].reshape(n_tp * experts, rows_q)
+    pick_block = (jnp.arange(n_tp * experts)[:, None] == at_block.reshape(1, -1)).astype(BF)
+    found = lax.dot_general(
+        spares, pick_block, (((0,), (0,)), ((), ())), preferred_element_type=F32
+    )
+    lane = jnp.arange(rows_q)[:, None] == within.reshape(1, -1)
+    grad_weights = jnp.sum(jnp.where(lane, found, 0.0), axis=0).astype(BF)
+    grad_weights = grad_weights.reshape(top_count, local_tokens).T
     grad_tokens = lax.all_gather(feature_part, "tp", axis=1, tiled=True)
     return (grad_tokens, grad_weights, grad_gate[None], grad_up[None], grad_down[None])
 

time: 125 us -> 113 us (0.904)
  blocking collectives: 8.63 us -> 29.5 us
  waiting for transfers between devices: 50.9 us -> 32.9 us
  starting transfers between devices: 21.8 us -> 11.7 us
  other arithmetic: 6.12 us -> 1.66 us
  Pallas kernels: 0 us -> 3.03 us
  matrix products: 30.5 us -> 28.9 us
    all_to_all x0 -> x1, blocking collectives: none -> 21.9 us  [on_device(): lax.all_to_all(send_rows, 'ep', split_axis=0, concat_axis=0, tiled=True)]
    all_to_all x1 -> x0, waiting for transfers between devices: 13.3 us -> none  [on_device(): lax.all_to_all(send_rows, 'ep', split_axis=0, concat_axis=0, tiled=True)]
    all_to_all x1 -> x0, starting transfers between devices: 7.28 us -> none  [on_device(): lax.all_to_all(send_rows, 'ep', split_axis=0, concat_axis=0, tiled=True)]
    all_to_all x1, waiting for transfers between devices: 13.1 us -> 6.05 us  [on_device(): lax.all_to_all(send_back, 'ep', split_axis=0, concat_axis=0, tiled=True)]
    dot_general x2 -> x1, matrix products: 3.38 us -> 0.19 us  [on_device(): lax.dot_general(spares, pick_block, (((0,), (0,)), ((), ())), preferred_e...]
    pallas_call x0 -> x1, Pallas kernels: none -> 3.03 us  [dispatch(): pl.pallas_call(body, name='dispatch', in_specs=[pl.BlockSpec(memory_space...]
    ppermute x9, waiting for transfers between devices: 18.4 us -> 21.3 us  [swap(): return lax.ppermute(x, 'tp', [(i, i ^ mask) for i in range(n)])]
    ppermute x9, starting transfers between devices: 5.86 us -> 3.27 us  [swap(): return lax.ppermute(x, 'tp', [(i, i ^ mask) for i in range(n)])]
  transfers between devices with their start and end apart: 12 -> 11, of which waited for: 5 -> 6; matrix products, arithmetic and copies ran while one was open for 20% -> 22% of each run, Pallas kernels for 0% -> 0%
where the time goes in v2:
time: 113 us
  waiting for transfers between devices  32.9 us (29%)
  blocking collectives  29.5 us (26%)
  matrix products  28.9 us (26%)
  starting transfers between devices  11.7 us (10%)
  local copies, waits for them, and re-layouts  4.14 us (4%)
  Pallas kernels  3.03 us (3%)
  other arithmetic  1.66 us (1%)
    all_to_all x1, blocking collectives, on_device(): lax.all_to_all(send_rows, 'ep', split_axis=0, concat_axis=0, tiled=True)  21.9 us
    ppermute x9, waiting for transfers between devices, swap(): return lax.ppermute(x, 'tp', [(i, i ^ mask) for i in range(n)])  21.3 us
    all_gather x1, blocking collectives, on_device(): grad_tokens = lax.all_gather(feature_part, 'tp', axis=1, tiled=True)  7.58 us
    all_to_all x1, waiting for transfers between devices, on_device(): lax.all_to_all(send_back, 'ep', split_axis=0, concat_axis=0, tiled=True)  6.05 us
    all_to_all x1, waiting for transfers between devices, on_device(): home = lax.all_to_all(share, 'ep', split_axis=1, concat_axis=1, tiled=True)  5.57 us
    all_to_all x1, starting transfers between devices, on_device(): home = lax.all_to_all(share, 'ep', split_axis=1, concat_axis=1, tiled=True)  4.8 us
    dot_general x1, matrix products, on_device(): along = jnp.einsum('rd,fd->rf', back, wdown, preferred_element_type=F32)  4.56 us
    dot_general x1, matrix products, on_device(): jnp.einsum('rd,rf->df', rows, gate_grad, preferred_element_type=F32)  4.28 us
  transfers between devices with their start and end apart: 11, of which 6 were waited for; matrix products, arithmetic and copies ran while one was open for 22% of the time, Pallas kernels for 0%

profile of v2, /device:TPU:0, one launch (start us, length us, event | category | flops | bytes accessed | tf_op | source)
XLA Modules:
  0.0 112.7 jit_solution(15764144485707675526)
XLA Ops:
  0.7 3.0 %dispatch.1 = (bf16[128,2048]{1,0:T(8,128)(2,1)}, bf16[128,2048]{1,0:T(8,128)(2,1)}, s32[2,192]{1,0:T(2,128)}) custom-call(s32[1]{0:T(128)} %bitcast.me_ref, s32[2,192]{1,0:T(2,128)} %bitcast.111, f32[2,192]{1,0:T(2,128)} %bitcast.112, bf16[192,2048]{1,0:T(8,128)(2,1)} %tok_ref.1, bf16[192,2048]{1,0:T(8,128)(2,1)} %cot_ref.1), custom_call_target="tpu_custom_call" | custom-call | tf_op jit(solution)/shard_map/dispatch/pallas_call | solution.py:76
  3.7 21.9 %all_to_all.15 = bf16[8,16,2048]{2,1,0:T(8,128)(2,1)S(1)} all-to-all(bf16[8,16,2048]{2,1,0:T(8,128)(2,1)} %bitcast.110), channel_id=1, replica_groups=mesh['ep'=8,'tp'=4] {'ep'}, dimensions={0} | all-to-all | bytes 1048576 | tf_op jit(solution)/shard_map/all_to_all | solution.py:112
  25.6 1.5 %collective-permute-start.2 = (bf16[128,2048]{1,0:T(8,128)(2,1)S(1)}, bf16[128,2048]{1,0:T(8,128)(2,1)}, u32[]{:S(2)}, u32[]{:S(2)}) collective-permute-start(bf16[128,2048]{1,0:T(8,128)(2,1)S(1)} %bitcast.97), channel_id=1, source_target_pairs={{0,2},{1,3},{2,0},{3,1},{4,6},{5,7},{6,4},{7,5},{8,10},{9,11},{10,... | collective-permute-start | bytes 1572872 | tf_op jit(solution)/shard_map/ppermute | solution.py:14
  27.2 3.6 %all-to-all-start = ((bf16[8,16,2048]{2,1,0:T(8,128)(2,1)}), bf16[8,16,2048]{2,1,0:T(8,128)(2,1)S(1)}, u32[]{:S(2)}, u32[]{:S(2)}) async-start(bf16[8,16,2048]{2,1,0:T(8,128)(2,1)} %bitcast.108), calls=%async_computation | async-start | bytes 1048576 | tf_op jit(solution)/shard_map/all_to_all | solution.py:113
  30.8 7.5 %collective-permute-done.2 = bf16[128,2048]{1,0:T(8,128)(2,1)} collective-permute-done((bf16[128,2048]{1,0:T(8,128)(2,1)S(1)}, bf16[128,2048]{1,0:T(8,128)(2,1)}, u32[]{:S(2)}, u32[]{:S(2)}) %collective-permute-start.2) | collective-permute-done | bytes 524320 | tf_op jit(solution)/shard_map/ppermute | solution.py:14
  38.6 6.1 %all-to-all-done = bf16[8,16,2048]{2,1,0:T(8,128)(2,1)S(1)} async-done(((bf16[8,16,2048]{2,1,0:T(8,128)(2,1)}), bf16[8,16,2048]{2,1,0:T(8,128)(2,1)S(1)}, u32[]{:S(2)}, u32[]{:S(2)}) %all-to-all-start) | async-done | bytes 524320 | tf_op jit(solution)/shard_map/all_to_all | solution.py:113
  44.7 0.5 collective-permute-start
  45.2 3.9 %fusion.7 = f32[512,512]{1,0:T(8,128)} fusion(bf16[1,2048,512]{2,1,0:T(8,128)(2,1)S(1)} %copy-done, bf16[128,2048]{1,0:T(8,128)(2,1)} %collective-permute-done.3, bf16[128,2048]{1,0:T(8,128)(2,1)} %collective-permute-done.2, bf16[128,2048]{1,0:T(8,128)(2,1)} %collective-permute-done.1, bf16[128,2048]{1,0:T(8,128)(2,1)S(1)} %bitcast.99), kind=kOutput, calls=%fused_computation.16 | convolution fusion | flops 1082130432 | bytes 5242880 | tf_op jit(solution)/shard_map/dot_general | solution.py:118
  49.1 3.6 %fusion.5 = f32[512,512]{1,0:T(8,128)} fusion(bf16[1,2048,512]{2,1,0:T(8,128)(2,1)S(1)} %copy-done.1, bf16[128,2048]{1,0:T(8,128)(2,1)} %collective-permute-done.3, bf16[128,2048]{1,0:T(8,128)(2,1)} %collective-permute-done.2, bf16[128,2048]{1,0:T(8,128)(2,1)} %collective-permute-done.1, bf16[128,2048]{1,0:T(8,128)(2,1)S(1)} %bitcast.100), kind=kOutput, calls=%fused_computation.14 | convolution fusion | flops 1082130432 | bytes 5242880 | tf_op jit(solution)/shard_map/dot_general | solution.py:119
  52.7 4.3 %collective-permute-done = bf16[128,2048]{1,0:T(8,128)(2,1)} collective-permute-done((bf16[128,2048]{1,0:T(8,128)(2,1)S(1)}, bf16[128,2048]{1,0:T(8,128)(2,1)}, u32[]{:S(2)}, u32[]{:S(2)}) %collective-permute-start) | collective-permute-done | bytes 524320 | tf_op jit(solution)/shard_map/ppermute | solution.py:14
  57.0 1.6 %pad_maximum_fusion = bf16[512,2048]{1,0:T(8,128)(2,1)S(1)} fusion(bf16[128,2048]{1,0:T(8,128)(2,1)} %collective-permute-done.3, bf16[128,2048]{1,0:T(8,128)(2,1)} %collective-permute-done.2, bf16[128,2048]{1,0:T(8,128)(2,1)} %collective-permute-done.1, bf16[128,2048]{1,0:T(8,128)(2,1)S(1)} %bitcast.101), kind=kLoop, calls=%fused_computation.10 | loop fusion | flops 8388608 | bytes 4194304 | tf_op jit(solution)/shard_map/concatenate | solution.py:114
  58.7 0.5 collective-permute-done.5
  59.2 4.6 %multiply_reduce_fusion = (bf16[512]{0:T(512)(128)(2,1)S(1)}, bf16[512,512]{1,0:T(8,128)(2,1)S(1)}, bf16[512,512]{1,0:T(8,128)(2,1)S(1)}) fusion(f32[512,512]{1,0:T(8,128)} %fusion.5, f32[512,512]{1,0:T(8,128)} %fusion.7, f32[512]{0:T(512)S(1)} %reshape.92, bf16[1,512,2048]{2,1,0:T(8,128)(2,1)} %param.13, bf16[128,2048]{1,0:T(8,128)(2,1)} %collective-permute-done.5, ...), kind=kOutput, calls=%fused_computation.37 | convolution fusion | flops 1086586368 | bytes 7343104 | tf_op jit(solution)/shard_map/rd,fd->rf/dot_general | solution.py:134
  63.9 0.5 fusion.18
  64.4 1.1 copy-done.2
  65.5 0.5 fusion.14
  66.2 0.5 fusion.26
  66.6 0.5 fusion.11
  67.6 0.5 fusion.23
  68.1 0.6 add_convert_fusion.1
  68.7 0.6 collective-permute-start.8
  69.2 4.0 %fusion.1 = bf16[1,2048,512]{2,1,0:T(8,128)(2,1)} fusion(bf16[512,512]{1,0:T(8,128)(2,1)S(1)} %get-tuple-element.26, bf16[128,2048]{1,0:T(8,128)(2,1)} %collective-permute-done.3, bf16[128,2048]{1,0:T(8,128)(2,1)} %collective-permute-done.2, bf16[128,2048]{1,0:T(8,128)(2,1)} %collective-permute-done.1, bf16[128,2048]{1,0:T(8,128)(2,1)S(1)} %bitcast.103), kind=kOutput, calls=%fused_computation.4 | convolution fusion | flops 1083179008 | bytes 4718592 | tf_op jit(solution)/shard_map/rd,rf->df/dot_general | solution.py:167
  73.7 9.0 %collective-permute-done.8 = bf16[512,512]{1,0:T(8,128)(2,1)S(1)} collective-permute-done((bf16[512,512]{1,0:T(8,128)(2,1)S(1)}, bf16[512,512]{1,0:T(8,128)(2,1)S(1)}, u32[]{:S(2)}, u32[]{:S(2)}) %collective-permute-start.8) | collective-permute-done | bytes 524320 | tf_op jit(solution)/shard_map/ppermute | solution.py:14
  82.7 0.6 add_convert_fusion
  83.4 0.8 copy.21
  84.2 4.8 %all-to-all-start.2 = ((bf16[4,8,16,512]{3,2,0,1:T(8,128)(2,1)}), bf16[4,8,16,512]{3,2,0,1:T(8,128)(2,1)S(1)}, u32[]{:S(2)}, u32[]{:S(2)}) async-start(bf16[4,8,16,512]{3,2,0,1:T(8,128)(2,1)} %copy.21), calls=%async_computation.2 | async-start | bytes 1048576 | tf_op jit(solution)/shard_map/all_to_all | solution.py:164
  89.0 4.3 %fusion = bf16[1,2048,512]{2,1,0:T(8,128)(2,1)} fusion(bf16[512,512]{1,0:T(8,128)(2,1)S(1)} %get-tuple-element.25, bf16[128,2048]{1,0:T(8,128)(2,1)} %collective-permute-done.3, bf16[128,2048]{1,0:T(8,128)(2,1)} %collective-permute-done.2, bf16[128,2048]{1,0:T(8,128)(2,1)} %collective-permute-done.1, bf16[128,2048]{1,0:T(8,128)(2,1)} %bitcast.102), kind=kOutput, calls=%fused_computation.3 | convolution fusion | flops 1083179008 | bytes 4718592 | tf_op jit(solution)/shard_map/rd,rf->df/dot_general | solution.py:166
  93.3 4.1 %fusion.2 = bf16[1,512,2048]{2,1,0:T(8,128)(2,1)} fusion(f32[512]{0:T(512)S(1)} %reshape.92, f32[512,512]{1,0:T(8,128)S(1)} %copy-done.10, bf16[128,2048]{1,0:T(8,128)(2,1)} %collective-permute-done.5, bf16[128,2048]{1,0:T(8,128)(2,1)} %collective-permute-done, bf16[128,2048]{1,0:T(8,128)(2,1)} %collective-permute-done.4, ...), kind=kOutput, calls=%fused_computation.5 | convolution fusion | flops 1085014016 | bytes 6293504 | tf_op jit(solution)/shard_map/rf,rd->fd/dot_general | solution.py:168
  97.4 5.6 %all-to-all-done.2 = bf16[4,8,16,512]{3,2,0,1:T(8,128)(2,1)S(1)} async-done(((bf16[4,8,16,512]{3,2,0,1:T(8,128)(2,1)}), bf16[4,8,16,512]{3,2,0,1:T(8,128)(2,1)S(1)}, u32[]{:S(2)}, u32[]{:S(2)}) %all-to-all-start.2) | async-done | bytes 524320 | tf_op jit(solution)/shard_map/all_to_all | solution.py:164
  103.2 0.6 convert_element_type.124
  104.2 7.6 %all_gather.3 = bf16[192,2048]{1,0:T(8,128)(2,1)S(1)} all-gather(bf16[192,512]{1,0:T(8,128)(2,1)S(1)} %convolution_convert_fusion.3), channel_id=1, replica_groups=mesh['ep'=8,'tp'=4] {'tp'}, dimensions={1}, use_global_device_ids=true | all-gather | bytes 983040 | tf_op jit(solution)/shard_map/all_gather | solution.py:187
  111.8 0.9 copy.30
  (51 shorter events, 2.4 us)
Async XLA Ops:
  0.6 44.5 %copy-start = (bf16[1,2048,512]{2,1,0:T(8,128)(2,1)S(1)}, bf16[1,2048,512]{2,1,0:T(8,128)(2,1)}, u32[]{:S(2)}) copy-start(bf16[1,2048,512]{2,1,0:T(8,128)(2,1)} %param.11) | copy-start | bytes 6291460
  0.6 37.8 %copy-start.7 = (s32[192,2]{0,1:T(2,128)S(1)}, s32[192,2]{0,1:T(2,128)}, u32[]{:S(2)}) copy-start(s32[192,2]{0,1:T(2,128)} %param.9) | copy-start | bytes 4612
  3.7 34.7 %copy-start.8 = (s32[2,192]{1,0:T(2,128)S(1)}, s32[2,192]{1,0:T(2,128)}, u32[]{:S(2)}) copy-start(s32[2,192]{1,0:T(2,128)} %get-tuple-element.13) | copy-start | bytes 4612
  25.6 31.3 %copy-start.3 = (bf16[8,16,2048]{2,1,0:T(8,128)(2,1)}, bf16[8,16,2048]{2,1,0:T(8,128)(2,1)S(1)}, u32[]{:S(2)}) copy-start(bf16[8,16,2048]{2,1,0:T(8,128)(2,1)S(1)} %all_to_all.15) | copy-start | bytes 1572868
  25.6 12.6 %collective-permute-start.2 = (bf16[128,2048]{1,0:T(8,128)(2,1)S(1)}, bf16[128,2048]{1,0:T(8,128)(2,1)}, u32[]{:S(2)}, u32[]{:S(2)}) collective-permute-start(bf16[128,2048]{1,0:T(8,128)(2,1)S(1)} %bitcast.97), channel_id=1, source_target_pairs={{0,2},{1,3},{2,0},{3,1},{4,6},{5,7},{6,4},{7,5},{8,10},{9,11},{10,... | collective-permute-start | bytes 1572872 | tf_op jit(solution)/shard_map/ppermute | solution.py:14
  27.2 17.5 %all-to-all-start = ((bf16[8,16,2048]{2,1,0:T(8,128)(2,1)}), bf16[8,16,2048]{2,1,0:T(8,128)(2,1)S(1)}, u32[]{:S(2)}, u32[]{:S(2)}) async-start(bf16[8,16,2048]{2,1,0:T(8,128)(2,1)} %bitcast.108), calls=%async_computation | async-start | bytes 1048576 | tf_op jit(solution)/shard_map/all_to_all | solution.py:113
  30.8 14.4 %collective-permute-start.1 = (bf16[128,2048]{1,0:T(8,128)(2,1)S(1)}, bf16[128,2048]{1,0:T(8,128)(2,1)}, u32[]{:S(2)}, u32[]{:S(2)}) collective-permute-start(bf16[128,2048]{1,0:T(8,128)(2,1)S(1)} %bitcast.98), channel_id=1, source_target_pairs={{0,1},{1,0},{2,3},{3,2},{4,5},{5,4},{6,7},{7,6},{8,9},{9,8},{10,11... | collective-permute-start | bytes 1572872 | tf_op jit(solution)/shard_map/ppermute | solution.py:14
  38.3 6.9 %collective-permute-start.3 = (bf16[128,2048]{1,0:T(8,128)(2,1)}, bf16[128,2048]{1,0:T(8,128)(2,1)}, u32[]{:S(2)}, u32[]{:S(2)}) collective-permute-start(bf16[128,2048]{1,0:T(8,128)(2,1)} %collective-permute-done.2), channel_id=1, source_target_pairs={{0,1},{1,0},{2,3},{3,2},{4,5},{5,4},{6,7},{7,6},{8,9},{9,8},{10,11... | collective-permute-start | bytes 1572872 | tf_op jit(solution)/shard_map/ppermute | solution.py:14
  44.6 4.4 %copy-start.5 = (bf16[8,16,2048]{2,1,0:T(8,128)(2,1)}, bf16[8,16,2048]{2,1,0:T(8,128)(2,1)S(1)}, u32[]{:S(2)}) copy-start(bf16[8,16,2048]{2,1,0:T(8,128)(2,1)S(1)} %all-to-all-done) | copy-start | bytes 1572868
  44.7 4.4 %copy-start.1 = (bf16[1,2048,512]{2,1,0:T(8,128)(2,1)S(1)}, bf16[1,2048,512]{2,1,0:T(8,128)(2,1)}, u32[]{:S(2)}) copy-start(bf16[1,2048,512]{2,1,0:T(8,128)(2,1)} %param.12) | copy-start | bytes 6291460
  44.7 12.3 %collective-permute-start = (bf16[128,2048]{1,0:T(8,128)(2,1)S(1)}, bf16[128,2048]{1,0:T(8,128)(2,1)}, u32[]{:S(2)}, u32[]{:S(2)}) collective-permute-start(bf16[128,2048]{1,0:T(8,128)(2,1)S(1)} %bitcast.104), channel_id=1, source_target_pairs={{0,2},{1,3},{2,0},{3,1},{4,6},{5,7},{6,4},{7,5},{8,10},{9,11},{10,... | collective-permute-start | bytes 1572872 | tf_op jit(solution)/shard_map/ppermute | solution.py:14
  49.1 9.6 %collective-permute-start.4 = (bf16[128,2048]{1,0:T(8,128)(2,1)S(1)}, bf16[128,2048]{1,0:T(8,128)(2,1)}, u32[]{:S(2)}, u32[]{:S(2)}) collective-permute-start(bf16[128,2048]{1,0:T(8,128)(2,1)S(1)} %bitcast.105), channel_id=1, source_target_pairs={{0,1},{1,0},{2,3},{3,2},{4,5},{5,4},{6,7},{7,6},{8,9},{9,8},{10,11... | collective-permute-start | bytes 1572872 | tf_op jit(solution)/shard_map/ppermute | solution.py:14
  57.0 2.3 %collective-permute-start.5 = (bf16[128,2048]{1,0:T(8,128)(2,1)}, bf16[128,2048]{1,0:T(8,128)(2,1)}, u32[]{:S(2)}, u32[]{:S(2)}) collective-permute-start(bf16[128,2048]{1,0:T(8,128)(2,1)} %collective-permute-done), channel_id=1, source_target_pairs={{0,1},{1,0},{2,3},{3,2},{4,5},{5,4},{6,7},{7,6},{8,9},{9,8},{10,11... | collective-permute-start | bytes 1572872 | tf_op jit(solution)/shard_map/ppermute | solution.py:14
  63.9 1.6 %copy-start.2 = (bf16[1,2048,512]{2,1,0:T(8,128)(2,1)S(1)}, bf16[1,2048,512]{2,1,0:T(8,128)(2,1)}, u32[]{:S(2)}) copy-start(bf16[1,2048,512]{2,1,0:T(8,128)(2,1)} %param.12) | copy-start | bytes 6291460
  65.9 2.1 %collective-permute-start.7 = (bf16[512,512]{1,0:T(8,128)(2,1)S(1)}, bf16[512,512]{1,0:T(8,128)(2,1)S(1)}, u32[]{:S(2)}, u32[]{:S(2)}) collective-permute-start(bf16[512,512]{1,0:T(8,128)(2,1)S(1)} %fusion.14), channel_id=1, source_target_pairs={{0,1},{1,0},{2,3},{3,2},{4,5},{5,4},{6,7},{7,6},{8,9},{9,8},{10,11... | collective-permute-start | bytes 1572872 | tf_op jit(solution)/shard_map/ppermute | solution.py:14
  67.1 6.6 %collective-permute-start.6 = (bf16[512,512]{1,0:T(8,128)(2,1)S(1)}, bf16[512,512]{1,0:T(8,128)(2,1)S(1)}, u32[]{:S(2)}, u32[]{:S(2)}) collective-permute-start(bf16[512,512]{1,0:T(8,128)(2,1)S(1)} %fusion.11), channel_id=1, source_target_pairs={{0,1},{1,0},{2,3},{3,2},{4,5},{5,4},{6,7},{7,6},{8,9},{9,8},{10,11... | collective-permute-start | bytes 1572872 | tf_op jit(solution)/shard_map/ppermute | solution.py:14
  68.0 1.2 %copy-start.4 = (bf16[8,16,2048]{2,1,0:T(8,128)(2,1)S(1)}, bf16[8,16,2048]{2,1,0:T(8,128)(2,1)}, u32[]{:S(2)}) copy-start(bf16[8,16,2048]{2,1,0:T(8,128)(2,1)} %copy-done.3) | copy-start | bytes 1572868
  68.7 14.0 %collective-permute-start.8 = (bf16[512,512]{1,0:T(8,128)(2,1)S(1)}, bf16[512,512]{1,0:T(8,128)(2,1)S(1)}, u32[]{:S(2)}, u32[]{:S(2)}) collective-permute-start(bf16[512,512]{1,0:T(8,128)(2,1)S(1)} %add_convert_fusion.1), channel_id=1, source_target_pairs={{0,2},{1,3},{2,0},{3,1},{4,6},{5,7},{6,4},{7,5},{8,10},{9,11},{10,... | collective-permute-start | bytes 1572872 | tf_op jit(solution)/shard_map/ppermute | solution.py:14
  84.2 18.8 %all-to-all-start.2 = ((bf16[4,8,16,512]{3,2,0,1:T(8,128)(2,1)}), bf16[4,8,16,512]{3,2,0,1:T(8,128)(2,1)S(1)}, u32[]{:S(2)}, u32[]{:S(2)}) async-start(bf16[4,8,16,512]{3,2,0,1:T(8,128)(2,1)} %copy.21), calls=%async_computation.2 | async-start | bytes 1048576 | tf_op jit(solution)/shard_map/all_to_all | solution.py:164
  89.0 4.3 %copy-start.6 = (bf16[8,16,2048]{2,1,0:T(8,128)(2,1)S(1)}, bf16[8,16,2048]{2,1,0:T(8,128)(2,1)}, u32[]{:S(2)}) copy-start(bf16[8,16,2048]{2,1,0:T(8,128)(2,1)} %copy-done.5) | copy-start | bytes 1572868
  89.0 4.3 %copy-start.9 = (f32[512,512]{1,0:T(8,128)S(1)}, f32[512,512]{1,0:T(8,128)}, u32[]{:S(2)}) copy-start(f32[512,512]{1,0:T(8,128)} %fusion.7) | copy-start | bytes 3145732
  89.0 4.3 %copy-start.10 = (f32[512,512]{1,0:T(8,128)S(1)}, f32[512,512]{1,0:T(8,128)}, u32[]{:S(2)}) copy-start(f32[512,512]{1,0:T(8,128)} %fusion.5) | copy-start | bytes 3145732
